TPU v7x, 256 devices: a whole 4x4x8 slice. The times are simulated.
256 devices in a mesh: sp: 64 (over z, x, core), tp: 4 (over y).
Axes of the slice: x: 4, y: 4, z: 8, core: 2. Of those that a mesh axis runs over, the one named last changes fastest.
Arguments:
- stream: bfloat16 [8192, 2048], P(('sp', 'tp')), may hold values from -2.5 to 2.5
- recurrence_input: bfloat16 [8192, 2, 1024], P('sp', None, 'tp'), may hold values from -6 to 6
- output_gate_input: bfloat16 [8192, 2, 1024], P('sp', None, 'tp'), may hold values from -6 to 6
- convolution_taps: bfloat16 [4, 2, 1024], P(None, None, 'tp'), may hold values from -4 to 4
- first_group_gates: bfloat16 [2, 16, 64, 64], P(None, 'tp'), may hold values from -0.75 to 0.75
- second_group_gates: bfloat16 [2, 8, 128, 128], P(None, 'tp'), may hold values from -0.5 to 0.5
- channel_decay: float32 [2, 1024], P(None, 'tp'), may hold values from 4.7 to 13.6
- position_log_extra: float32 [8192, 2, 1024], P('sp', None, 'tp'), may hold values from -1.4 to 0, as said below
- recurrence_output_weight: bfloat16 [2, 1024, 2048], P(None, 'tp'), may hold values from -0.125 to 0.125
- first_norm_gain: float32 [2048], replicated, may hold values from 0.1 to 1.9
- first_norm_bias: float32 [2048], replicated, may hold values from -1.75 to 1.75
- routed_expert_index: int32 [8192, 4], P('sp'), may hold values from 0 to 63, all different within a row; in each aligned block of 32 rows (0 to 31, 32 to 63, ...) at most 2 rows name the same one
- routed_expert_weight: float32 [8192, 4], P('sp'), may hold values from 0.25 to 1
- routed_gate_weight: bfloat16 [64, 2048, 512], P('sp', None, 'tp'), may hold values from -0.125 to 0.125
- routed_up_weight: bfloat16 [64, 2048, 512], P('sp', None, 'tp'), may hold values from -0.125 to 0.125
- routed_down_weight: bfloat16 [64, 512, 2048], P('sp', 'tp'), may hold values from -0.25 to 0.25
- shared_gate_weight: bfloat16 [2048, 512], replicated, may hold values from -0.125 to 0.125
- shared_up_weight: bfloat16 [2048, 512], replicated, may hold values from -0.125 to 0.125
- shared_down_weight: bfloat16 [512, 2048], replicated, may hold values from -0.25 to 0.25
- second_norm_gain: float32 [2048], replicated, may hold values from 0.1 to 1.9
- second_norm_bias: float32 [2048], replicated, may hold values from -1.75 to 1.75
Outputs:
- result: bfloat16 [8192, 2048], P(('sp', 'tp'))
Inputs may be any that keep to these rules, and one draw needn't show every extreme that they name: `routed_expert_index`: each row names 4 different experts. In each aligned block of 32 rows no expert is named more than 2 times, and in some block an expert is named exactly 2 times. `position_log_extra`: every entry is negative.
All inputs are finite; a program needn't handle non-finite values.
Results may differ from a plain program's by a relative error of at most 0.015.
Values may be sent and summed in bfloat16 or wider, within the bound.
A program may use at most 64 MiB of HBM per device.

v0:
```python
import jax
import jax.numpy as jnp
from jax import lax
from jax.sharding import PartitionSpec as P

RESIDUAL_SCALE = 8.0**0.25
NORM_EPSILON = 1e-05


def copy_for_each(shard, axis):
    count = lax.axis_size(axis)
    return lax.all_to_all(
        jnp.broadcast_to(shard[None], (count, *shard.shape)), axis, 0, 0, tiled=True
    )


def all_in_one(shard, axis):
    leaves = jax.tree.leaves(shard)
    sequence = sorted(range(len(leaves)), key=lambda k: -leaves[k].size)
    width = (1, *leaves[sequence[0]].shape)[-1]
    lines = [
        jnp.pad(leaves[k].reshape(-1), (0, -leaves[k].size % width)).reshape(-1, width)
        for k in sequence
    ]
    both, at, found = (copy_for_each(jnp.concatenate(lines), axis), 0, {})
    for k, line in zip(sequence, lines):
        slab = both[:, at : at + len(line)].reshape(len(both), -1)
        found[k] = slab[:, : leaves[k].size].reshape(-1, *leaves[k].shape)
        at += len(line)
    numbers = iter(range(len(leaves)))
    return jax.tree.map(lambda _: found[next(numbers)], shard)


def joined_by_halves(pieces, combine):
    while len(jax.tree.leaves(pieces)[0]) > 1:
        pieces = jax.vmap(combine)(
            *(jax.tree.map(lambda part: part[side::2], pieces) for side in (0, 1))
        )
    return jax.tree.map(lambda part: part[0], pieces)


def entering(shard, axis, combine, identity):
    count, mine = (lax.axis_size(axis), lax.axis_index(axis))
    passed = jnp.arange(count) < mine

    def kept(part, zero, own):
        part = jnp.where(
            passed.reshape(-1, *(1 for _ in own.shape)), part, jnp.asarray(zero, own.dtype)
        )
        return part

    pieces = all_in_one(shard, axis)
    return joined_by_halves(jax.tree.map(kept, pieces, identity, shard), combine)


def shifted(shard, axis, by):
    count = lax.axis_size(axis)
    pairs = [(i, i + by) for i in range(count) if 0 <= i + by < count]
    return lax.ppermute(shard, axis, pairs)


def cut_along(shard, dim, count):
    dims = shard.shape
    pieces = shard.reshape(*dims[:dim], count, dims[dim] // count, *dims[dim + 1 :])
    return jnp.moveaxis(pieces, dim, 0)


def summed_on_arrival(shard, axis, dim):
    count = lax.axis_size(axis)
    pieces = lax.all_to_all(cut_along(shard, dim, count), axis, 0, 0, tiled=True)
    return jnp.sum(pieces.astype(jnp.float32), axis=0)


def layer_norm(values, gain_vec, bias_vec):
    row_mean = jnp.mean(values, axis=-1, keepdims=True)
    spread = jnp.mean(jnp.square(values - row_mean), axis=-1, keepdims=True)
    return (values - row_mean) * lax.rsqrt(spread + NORM_EPSILON) * gain_vec + bias_vec


def block_gates(conv_rows, weights, head_size):
    length = conv_rows.shape[0]
    head_rows = conv_rows.reshape(length, -1, head_size)
    pre_act = jnp.einsum("thc,ghcd->gthd", head_rows, weights, preferred_element_type=jnp.float32)
    gate_pair = jax.nn.sigmoid(pre_act).reshape(2, length, -1)
    return (gate_pair[0], gate_pair[1])


def chain_link(first_part, second_part):
    return (first_part[0] * second_part[0], second_part[0] * first_part[1] + second_part[1])


def carried(totals):
    unity = jnp.ones_like(totals[0])
    nought = jnp.zeros_like(totals[1])
    return entering(totals, "sp", chain_link, (unity, nought))[1]


def expert_terms(picked, letters, gate_w, up_w, down_w):
    gate_form = letters + "d,ldf->" + letters + "f"
    down_form = letters + "f,lfd->" + letters + "d"
    gated = jnp.einsum(gate_form, picked, gate_w, preferred_element_type=jnp.float32)
    lifted = jnp.einsum(gate_form, picked, up_w, preferred_element_type=jnp.float32)
    hidden = (jax.nn.silu(gated) * lifted).astype(jnp.bfloat16)
    return jnp.einsum(down_form, hidden, down_w, preferred_element_type=jnp.float32)


def shards(
    stream,
    recurrence_input,
    output_gate_input,
    convolution_taps,
    first_group_gates,
    second_group_gates,
    channel_decay,
    position_log_extra,
    recurrence_output_weight,
    first_norm_gain,
    first_norm_bias,
    routed_expert_index,
    routed_expert_weight,
    routed_gate_weight,
    routed_up_weight,
    routed_down_weight,
    shared_gate_weight,
    shared_up_weight,
    shared_down_weight,
    second_norm_gain,
    second_norm_bias,
):
    length = recurrence_input.shape[0]
    tap_count = convolution_taps.shape[0]
    border = shifted(recurrence_input[length - (tap_count - 1) :], "sp", 1)
    padded = jnp.concatenate([border, recurrence_input], axis=0).astype(jnp.float32)
    tap_weights = convolution_taps.astype(jnp.float32)
    summed = tap_weights[0] * padded[0:length]
    for offset in range(1, tap_count):
        summed = summed + tap_weights[offset] * padded[offset : offset + length]
    conv_rows = summed.astype(jnp.bfloat16)
    recur_a, input_a = block_gates(conv_rows[:, 0], first_group_gates, first_group_gates.shape[-1])
    recur_b, input_b = block_gates(
        conv_rows[:, 1], second_group_gates, second_group_gates.shape[-1]
    )
    recurrence_gate = jnp.stack([recur_a, recur_b], axis=1)
    input_gate = jnp.stack([input_a, input_b], axis=1)
    decay_logarithm = -8.0 * recurrence_gate * jax.nn.softplus(-channel_decay) + position_log_extra
    decay_rate = jnp.exp(decay_logarithm)
    driving = (
        jnp.sqrt(-jnp.expm1(2.0 * decay_logarithm)) * input_gate * conv_rows.astype(jnp.float32)
    )
    running = jnp.cumsum(decay_logarithm, axis=0)
    tail_sum = jnp.sum(jnp.exp(running[-1] - running) * driving, axis=0)
    incoming = carried((jnp.exp(running[-1]), tail_sum))
    opening = driving[:1] + decay_rate[:1] * incoming
    started = jnp.concatenate([opening, driving[1:]], axis=0)
    states = lax.associative_scan(chain_link, (decay_rate, started), axis=0)[1]
    branch_output = (jax.nn.gelu(output_gate_input.astype(jnp.float32)) * states).astype(
        jnp.bfloat16
    )
    tp_count = lax.axis_size("tp")
    quarter = length // tp_count
    mixed = summed_on_arrival(
        jnp.einsum(
            "tgc,gcd->td",
            branch_output,
            recurrence_output_weight,
            preferred_element_type=jnp.float32,
        ).astype(jnp.bfloat16),
        "tp",
        0,
    )
    normed = layer_norm(
        RESIDUAL_SCALE * stream.astype(jnp.float32) + mixed, first_norm_gain, first_norm_bias
    ).astype(jnp.bfloat16)
    width = normed.shape[1]
    top_count = routed_expert_index.shape[1]
    local_count = routed_gate_weight.shape[0]
    expert_count = local_count * lax.axis_size("sp")
    capacity = max(2, 5 * quarter * top_count // (4 * expert_count))
    block_ids = routed_expert_index.reshape(tp_count, quarter * top_count)
    onehot = (
        block_ids[:, :, None] == jnp.arange(expert_count, dtype=jnp.int32)[None, None, :]
    ).astype(jnp.int32)
    slot_ranks = jnp.sum((jnp.cumsum(onehot, axis=1) - onehot) * onehot, axis=2)
    own_index = lax.axis_index("tp")
    own_ids = lax.dynamic_index_in_dim(block_ids, own_index, 0, keepdims=False)
    own_ranks = lax.dynamic_index_in_dim(slot_ranks, own_index, 0, keepdims=False)
    blank_row = jnp.zeros((1, width), jnp.bfloat16)
    padded_rows = jnp.concatenate([normed, blank_row], axis=0)
    targets = own_ids * capacity + own_ranks
    sources = jnp.arange(quarter * top_count, dtype=jnp.int32) // top_count
    table = jnp.full((expert_count * capacity,), quarter, jnp.int32).at[targets].set(sources)
    outgoing = jnp.take(padded_rows, table, axis=0).reshape(expert_count, capacity, width)
    arrived = lax.all_to_all(outgoing, "sp", split_axis=0, concat_axis=0, tiled=True)
    slots = arrived.shape[1]
    fanned = lax.all_gather(arrived[None], "tp", axis=0, tiled=True)
    shaped = fanned.reshape(tp_count, -1, local_count, slots, width)
    partial_value = expert_terms(
        shaped, "xslc", routed_gate_weight, routed_up_weight, routed_down_weight
    )
    summed_rows = summed_on_arrival(partial_value.astype(jnp.bfloat16), "tp", 0)
    leaving = summed_rows.astype(jnp.bfloat16).reshape(-1, slots, width)
    returned = lax.all_to_all(leaving, "sp", split_axis=0, concat_axis=0, tiled=True)
    picked_rows = returned.reshape(expert_count * capacity, width)[own_ids * capacity + own_ranks]
    own_weights = lax.dynamic_slice_in_dim(routed_expert_weight, own_index * quarter, quarter, 0)
    routed = jnp.sum(
        own_weights[:, :, None]
        * picked_rows.reshape(quarter, top_count, width).astype(jnp.float32),
        axis=1,
    )
    shared_hidden = (
        jax.nn.silu(jnp.dot(normed, shared_gate_weight, preferred_element_type=jnp.float32))
        * jnp.dot(normed, shared_up_weight, preferred_element_type=jnp.float32)
    ).astype(jnp.bfloat16)
    shared_out = jnp.dot(shared_hidden, shared_down_weight, preferred_element_type=jnp.float32)
    final = layer_norm(
        RESIDUAL_SCALE * normed.astype(jnp.float32) + (shared_out + routed),
        second_norm_gain,
        second_norm_bias,
    )
    return final.astype(jnp.bfloat16)


def solution(mesh):
    in_specs = (
        P(("sp", "tp"), None),
        P("sp", None, "tp"),
        P("sp", None, "tp"),
        P(None, None, "tp"),
        P(None, "tp", None, None),
        P(None, "tp", None, None),
        P(None, "tp"),
        P("sp", None, "tp"),
        P(None, "tp", None),
        P(),
        P(),
        P("sp", None),
        P("sp", None),
        P("sp", None, "tp"),
        P("sp", None, "tp"),
        P("sp", "tp", None),
        P(),
        P(),
        P(),
        P(),
        P(),
    )
    out_specs = P(("sp", "tp"), None)
    return jax.shard_map(shards, mesh=mesh, in_specs=in_specs, out_specs=out_specs, check_vma=False)
```

profile of v0, /device:TPU:1, one launch (start us, length us, event | category | flops | bytes accessed | tf_op | source)
XLA Modules:
  0.0 205.7 jit_solution(793034132163294517)
XLA Ops:
  6.5 1.1 copy.130
  7.6 4.5 %collective-permute-start = (bf16[3,2,256]{2,0,1:T(4,128)(2,1)S(1)}, bf16[3,2,256]{2,0,1:T(4,128)(2,1)S(1)}, u32[]{:S(2)}, u32[]{:S(2)}) collective-permute-start(bf16[3,2,256]{2,0,1:T(4,128)(2,1)S(1)} %slice.395), channel_id=1, source_target_pairs={{0,4},{4,8},{8,12},{12,16},{16,20},{20,24},{24,28},{28,32},{32,36}... | collective-permute-start | bytes 9224 | tf_op jit(solution)/shard_map/ppermute | solution.py:59
  12.1 0.7 convert_element_type.67
  12.9 0.7 fusion.84
  13.6 0.8 copy.147
  14.4 0.7 reshape.136
  15.1 0.1 fusion.45
  15.2 0.1 copy.132
  15.4 0.3 fusion.20
  15.7 0.1 copy.138
  15.8 0.1 copy.134
  16.0 0.3 fusion.16
  16.3 0.1 copy.165
  16.4 1.0 fusion.101
  17.4 0.2 fusion.53
  17.6 0.6 slice_bitcast_fusion
  18.1 0.6 fusion.99
  18.7 0.1 copy.141
  18.8 0.8 copy.166
  19.6 1.2 fusion.52
  20.9 0.7 broadcast_in_dim.61
  21.6 11.3 %all-to-all-start = ((f32[64,4,256]{2,1,0:T(4,128)}), f32[64,4,256]{2,1,0:T(4,128)S(1)}, u32[]{:S(2)}, u32[]{:S(2)}) async-start(f32[64,4,256]{2,1,0:T(4,128)} %broadcast_in_dim.61), calls=%async_computation | async-start | bytes 524288 | tf_op jit(solution)/shard_map/all_to_all | solution.py:12
  32.9 0.8 fusion.60
  33.7 0.3 reduce_window_sum.23
  34.0 0.9 select_reduce_fusion
  34.9 0.7 fusion.90
  35.6 1.5 scatter_custom_fusion
  37.1 0.7 slice.345
  37.9 0.7 slice.343
  38.7 7.3 %all-to-all-done = f32[64,4,256]{2,1,0:T(4,128)S(1)} async-done(((f32[64,4,256]{2,1,0:T(4,128)}), f32[64,4,256]{2,1,0:T(4,128)S(1)}, u32[]{:S(2)}, u32[]{:S(2)}) %all-to-all-start) | async-done | bytes 262176 | tf_op jit(solution)/shard_map/all_to_all | solution.py:12
  46.0 0.1 fusion.103
  46.2 0.6 slice.315
  46.8 0.6 slice.316
  47.5 0.9 fusion.109
  49.0 1.0 fusion.106
  51.7 1.3 fusion.1
  53.0 4.3 %all-to-all-start.1 = ((bf16[4,32,2048]{2,1,0:T(8,128)(2,1)}), bf16[4,32,2048]{2,1,0:T(8,128)(2,1)S(1)}, u32[]{:S(2)}, u32[]{:S(2)}) async-start(bf16[4,32,2048]{2,1,0:T(8,128)(2,1)} %bitcast.17), calls=%async_computation.1 | async-start | bytes 1048576 | tf_op jit(solution)/shard_map/all_to_all | solution.py:70
  57.3 0.1 broadcast_in_dim.65
  57.5 8.8 %all-to-all-done.1 = bf16[4,32,2048]{2,1,0:T(8,128)(2,1)S(1)} async-done(((bf16[4,32,2048]{2,1,0:T(8,128)(2,1)}), bf16[4,32,2048]{2,1,0:T(8,128)(2,1)S(1)}, u32[]{:S(2)}, u32[]{:S(2)}) %all-to-all-start.1) | async-done | bytes 524320 | tf_op jit(solution)/shard_map/all_to_all | solution.py:70
  66.4 0.2 fusion.71
  66.6 0.2 multiply_reduce_fusion.2
  66.8 0.1 add_convert_fusion.1
  67.0 0.9 gather_fusion
  67.9 1.1 gather.10
  69.0 1.6 broadcast_select_fusion
  70.6 23.1 %all_to_all.25 = bf16[64,2,2048]{2,1,0:T(2,128)(2,1)S(1)} all-to-all(bf16[64,2,2048]{2,1,0:T(2,128)(2,1)S(1)} %broadcast_select_fusion), channel_id=1, replica_groups=mesh['sp'=64,'tp'=4] {'sp'}, dimensions={0} | all-to-all | bytes 1048576 | tf_op jit(solution)/shard_map/all_to_all | solution.py:193
  93.8 1.0 copy.148
  94.8 27.8 %all-gather.3.cloned.1.call-done = bf16[256,2,2048]{2,0,1:T(8,128)(2,1)} async-done(((bf16[64,2,2048]{2,0,1:T(8,128)(2,1)}), bf16[256,2,2048]{2,0,1:T(8,128)(2,1)}) %all-gather.3.cloned.1.call-update) | async-done | bytes 2097168 | tf_op jit(solution)/shard_map/all_gather | solution.py:195
  122.6 2.4 %fusion.7 = f32[4,64,1,2,128]{4,1,3,0,2:T(8,128)S(1)} fusion(bf16[4,64,2,2048]{3,1,0,2:T(8,128)(2,1)} %bitcast.118, bf16[1,2048,128]{2,1,0:T(8,128)(2,1)} %param.34), kind=kOutput, calls=%fused_computation.14 | convolution fusion | flops 268435456 | bytes 2883584 | tf_op jit(solution)/shard_map/xslcd,ldf->xslcf/dot_general | solution.py:101
  125.0 5.2 %fusion = bf16[4,1,64,1,2,2048]{5,2,4,3,1,0:T(8,128)(2,1)} fusion(bf16[4,64,2,2048]{3,1,0,2:T(8,128)(2,1)} %bitcast.119, bf16[1,128,2048]{2,1,0:T(8,128)(2,1)S(1)} %copy-done.2, bf16[1,2048,128]{2,1,0:T(8,128)(2,1)S(1)} %copy-done.3, f32[4,64,1,2,128]{4,1,3,0,2:T(8,128)S(1)} %fusion.7), kind=kOutput, calls=%fused_computation.4 | convolution fusion | flops 538312704 | bytes 5505024 | tf_op jit(solution)/shard_map/xslcf,lfd->xslcd/dot_general | solution.py:104
  130.2 28.9 %all_to_all.26 = bf16[4,1,64,1,2,2048]{5,2,4,3,1,0:T(8,128)(2,1)S(1)} all-to-all(bf16[4,1,64,1,2,2048]{5,2,4,3,1,0:T(8,128)(2,1)} %fusion), channel_id=1, replica_groups=mesh['sp'=64,'tp'=4] {'tp'}, dimensions={0} | all-to-all | bytes 4194304 | tf_op jit(solution)/shard_map/all_to_all | solution.py:70
  159.2 0.4 bitcast_reduce_fusion
  159.5 1.3 copy.153
  160.9 11.9 %all-to-all-start.4 = ((bf16[64,2,2048]{2,1,0:T(2,128)(2,1)}), bf16[64,2,2048]{2,1,0:T(2,128)(2,1)S(1)}, u32[]{:S(2)}, u32[]{:S(2)}) async-start(bf16[64,2,2048]{2,1,0:T(2,128)(2,1)} %copy.153), calls=%async_computation.4 | async-start | bytes 1048576 | tf_op jit(solution)/shard_map/all_to_all | solution.py:202
  172.9 0.1 copy.146
  173.0 2.7 %fusion.118 = f32[32,512]{1,0:T(8,128)} fusion(bf16[32,2048]{1,0:T(8,128)(2,1)S(1)} %add_convert_fusion.1, bf16[2048,512]{1,0:T(8,128)(2,1)} %param.37), kind=kOutput, calls=%fused_computation.192 | convolution fusion | flops 67108864 | bytes 2293760 | tf_op jit(solution)/shard_map/dot_general | solution.py:211
  175.6 14.8 %all-to-all-done.4 = bf16[64,2,2048]{2,1,0:T(2,128)(2,1)S(1)} async-done(((bf16[64,2,2048]{2,1,0:T(2,128)(2,1)}), bf16[64,2,2048]{2,1,0:T(2,128)(2,1)S(1)}, u32[]{:S(2)}, u32[]{:S(2)}) %all-to-all-start.4) | async-done | bytes 524320 | tf_op jit(solution)/shard_map/all_to_all | solution.py:202
  190.5 0.2 reshape.142
  190.7 1.7 gather_fusion.1
  192.4 1.4 reshape.143
  193.8 0.7 multiply_reduce_fusion
  194.5 3.3 %fusion.117 = (f32[32]{0:T(128)S(1)}, f32[32,2048]{1,0:T(8,128)S(1)}) fusion(f32[32,2048]{1,0:T(8,128)S(1)} %multiply_reduce_fusion, bf16[512,2048]{1,0:T(8,128)(2,1)} %param.39, bf16[32,2048]{1,0:T(8,128)(2,1)S(1)} %add_convert_fusion.1, bf16[2048,512]{1,0:T(8,128)(2,1)} %param.38, f32[32,512]{1,0:T(8,128)} %fusion.118), kind=kOutput, calls=%fused_computation.191 | convolution fusion | flops 134643680 | bytes 4915328 | tf_op jit(solution)/shard_map/dot_general | solution.py:214
  197.8 0.2 multiply_reduce_fusion.1
  198.0 0.8 add_convert_fusion
  (165 shorter events, 2.6 us)
Async XLA Ops:
  6.5 45.1 %copy-start = (bf16[2,256,2048]{2,1,0:T(8,128)(2,1)S(1)}, bf16[2,256,2048]{2,1,0:T(8,128)(2,1)}, u32[]{:S(2)}) copy-start(bf16[2,256,2048]{2,1,0:T(8,128)(2,1)} %param.29) | copy-start | bytes 6291460
  6.5 8.9 %copy-start.19 = (bf16[2,4,64,64]{3,2,1,0:T(8,128)(2,1)S(1)}, bf16[2,4,64,64]{3,2,1,0:T(8,128)(2,1)}, u32[]{:S(2)}) copy-start(bf16[2,4,64,64]{3,2,1,0:T(8,128)(2,1)} %param.25) | copy-start | bytes 196612
  7.6 7.4 %collective-permute-start = (bf16[3,2,256]{2,0,1:T(4,128)(2,1)S(1)}, bf16[3,2,256]{2,0,1:T(4,128)(2,1)S(1)}, u32[]{:S(2)}, u32[]{:S(2)}) collective-permute-start(bf16[3,2,256]{2,0,1:T(4,128)(2,1)S(1)} %slice.395), channel_id=1, source_target_pairs={{0,4},{4,8},{8,12},{12,16},{16,20},{20,24},{24,28},{28,32},{32,36}... | collective-permute-start | bytes 9224 | tf_op jit(solution)/shard_map/ppermute | solution.py:59
  12.8 2.5 %copy-start.7 = (f32[2,256]{1,0:T(2,128)}, f32[2,256]{1,0:T(2,128)S(1)}, u32[]{:S(2)}) copy-start(f32[2,256]{1,0:T(2,128)S(1)} %get-tuple-element.37) | copy-start | bytes 6148
  12.8 2.5 %copy-start.8 = (f32[2,256]{1,0:T(2,128)}, f32[2,256]{1,0:T(2,128)S(1)}, u32[]{:S(2)}) copy-start(f32[2,256]{1,0:T(2,128)S(1)} %get-tuple-element.38) | copy-start | bytes 6148
  12.8 2.5 %copy-start.9 = (f32[2,256]{1,0:T(2,128)}, f32[2,256]{1,0:T(2,128)S(1)}, u32[]{:S(2)}) copy-start(f32[2,256]{1,0:T(2,128)S(1)} %get-tuple-element.39) | copy-start | bytes 6148
  12.9 2.5 %copy-start.10 = (f32[2,256]{1,0:T(2,128)}, f32[2,256]{1,0:T(2,128)S(1)}, u32[]{:S(2)}) copy-start(f32[2,256]{1,0:T(2,128)S(1)} %get-tuple-element.40) | copy-start | bytes 6148
  15.0 0.9 copy-start.20
  19.6 1.2 copy-start.15
  21.6 24.4 %all-to-all-start = ((f32[64,4,256]{2,1,0:T(4,128)}), f32[64,4,256]{2,1,0:T(4,128)S(1)}, u32[]{:S(2)}, u32[]{:S(2)}) async-start(f32[64,4,256]{2,1,0:T(4,128)} %broadcast_in_dim.61), calls=%async_computation | async-start | bytes 524288 | tf_op jit(solution)/shard_map/all_to_all | solution.py:12
  35.6 12.9 %copy-start.17 = (s32[128]{0:T(128)}, s32[128]{0:T(128)S(1)}, u32[]{:S(2)}) copy-start(s32[128]{0:T(128)S(1)} %fusion.90) | copy-start | bytes 1540
  48.9 1.2 copy-start.5
  50.3 1.2 copy-start.6
  50.8 0.9 copy-start.4
  51.7 5.6 %copy-start.21 = (s32[128]{0:T(128)S(1)}, s32[128]{0:T(128)}, u32[]{:S(2)}) copy-start(s32[128]{0:T(128)} %scatter_custom_fusion) | copy-start | bytes 1540
  51.7 14.7 %copy-start.1 = (bf16[32,2048]{1,0:T(8,128)(2,1)S(1)}, bf16[32,2048]{1,0:T(8,128)(2,1)}, u32[]{:S(2)}) copy-start(bf16[32,2048]{1,0:T(8,128)(2,1)} %param.21) | copy-start | bytes 393220
  53.0 13.8 %copy-start.11 = (f32[2048]{0:T(1024)S(1)}, f32[2048]{0:T(1024)}, u32[]{:S(2)}) copy-start(f32[2048]{0:T(1024)} %param.31) | copy-start | bytes 24580
  53.0 13.8 %copy-start.12 = (f32[2048]{0:T(1024)S(1)}, f32[2048]{0:T(1024)}, u32[]{:S(2)}) copy-start(f32[2048]{0:T(1024)} %param.30) | copy-start | bytes 24580
  53.0 13.3 %all-to-all-start.1 = ((bf16[4,32,2048]{2,1,0:T(8,128)(2,1)}), bf16[4,32,2048]{2,1,0:T(8,128)(2,1)S(1)}, u32[]{:S(2)}, u32[]{:S(2)}) async-start(bf16[4,32,2048]{2,1,0:T(8,128)(2,1)} %bitcast.17), calls=%async_computation.1 | async-start | bytes 1048576 | tf_op jit(solution)/shard_map/all_to_all | solution.py:70
  57.3 65.3 %all-gather.3.cloned.1.call-start = ((), (), s32[]{:S(2)}) async-start(), calls=%async_computation.5 | async-start | bytes 2621440 | tf_op jit(solution)/shard_map/all_gather | solution.py:195
  94.7 30.2 %copy-start.2 = (bf16[1,128,2048]{2,1,0:T(8,128)(2,1)S(1)}, bf16[1,128,2048]{2,1,0:T(8,128)(2,1)}, u32[]{:S(2)}) copy-start(bf16[1,128,2048]{2,1,0:T(8,128)(2,1)} %param.36) | copy-start | bytes 1572868
  94.7 30.2 %copy-start.3 = (bf16[1,2048,128]{2,1,0:T(8,128)(2,1)S(1)}, bf16[1,2048,128]{2,1,0:T(8,128)(2,1)}, u32[]{:S(2)}) copy-start(bf16[1,2048,128]{2,1,0:T(8,128)(2,1)} %param.35) | copy-start | bytes 1572868
  159.2 13.6 %copy-start.16 = (f32[128,4]{0,1:T(4,128)S(1)}, f32[128,4]{0,1:T(4,128)}, u32[]{:S(2)}) copy-start(f32[128,4]{0,1:T(4,128)} %param.33) | copy-start | bytes 6148
  159.2 13.8 %copy-start.18 = (s32[128]{0:T(128)S(1)}, s32[128]{0:T(128)}, u32[]{:S(2)}) copy-start(s32[128]{0:T(128)} %copy-done.17) | copy-start | bytes 1540
  160.9 29.6 %all-to-all-start.4 = ((bf16[64,2,2048]{2,1,0:T(2,128)(2,1)}), bf16[64,2,2048]{2,1,0:T(2,128)(2,1)S(1)}, u32[]{:S(2)}, u32[]{:S(2)}) async-start(bf16[64,2,2048]{2,1,0:T(2,128)(2,1)} %copy.153), calls=%async_computation.4 | async-start | bytes 1048576 | tf_op jit(solution)/shard_map/all_to_all | solution.py:202
  194.5 3.5 %copy-start.13 = (f32[2048]{0:T(1024)S(1)}, f32[2048]{0:T(1024)}, u32[]{:S(2)}) copy-start(f32[2048]{0:T(1024)} %param.41) | copy-start | bytes 24580
  194.5 3.5 %copy-start.14 = (f32[2048]{0:T(1024)S(1)}, f32[2048]{0:T(1024)}, u32[]{:S(2)}) copy-start(f32[2048]{0:T(1024)} %param.40) | copy-start | bytes 24580
Sparse Core Ops, SparseCore 0:
  94.9 27.6 all-gather.2
where the time goes:
time: 207 us; the launch traced here: 206 us
  waiting for transfers between devices  58.8 us (28%)
  blocking collectives  52.1 us (25%)
  starting transfers between devices  32 us (15%)
  local copies, waits for them, and re-layouts  19.8 us (10%)
  matrix products  15.4 us (7%)
  between operations  14.3 us (7%)
  other arithmetic  13.3 us (6%)
    all_to_all x1, blocking collectives, summed_on_arrival(): lax.all_to_all(cut_along(shard, dim, count), axis, 0, 0, tiled=True)  28.9 us
    all_gather x1, waiting for transfers between devices, shards(): fanned = lax.all_gather(arrived[None], 'tp', axis=0, tiled=True)  27.8 us
    all_to_all x1, blocking collectives, shards(): lax.all_to_all(outgoing, 'sp', split_axis=0, concat_axis=0, tiled=True)  23.1 us
    all_to_all x1, waiting for transfers between devices, shards(): lax.all_to_all(leaving, 'sp', split_axis=0, concat_axis=0, tiled=True)  14.8 us
    all_to_all x1, starting transfers between devices, shards(): lax.all_to_all(leaving, 'sp', split_axis=0, concat_axis=0, tiled=True)  11.9 us
    all_to_all x1, starting transfers between devices, copy_for_each(): lax.all_to_all(jnp.broadcast_to(shard[None], (count, *shard.shape)), axis...  11.3 us
    all_to_all x1, waiting for transfers between devices, summed_on_arrival(): lax.all_to_all(cut_along(shard, dim, count), axis, 0, 0, tiled=True)  8.83 us
    all_to_all x1, waiting for transfers between devices, copy_for_each(): lax.all_to_all(jnp.broadcast_to(shard[None], (count, *shard.shape)), axis...  7.34 us
  transfers between devices with their start and end apart: 5, of which 4 were waited for; matrix products, arithmetic and copies ran while one was open for 6% of the time, Pallas kernels for 0%

commit v1 on v0

--- a/solution.py
+++ b/solution.py
@@ -5,6 +5,11 @@
 
 RESIDUAL_SCALE = 8.0**0.25
 NORM_EPSILON = 1e-05
+
+
+def tiled_gather(value, axis, dim):
+    copies = jnp.concatenate([value] * lax.axis_size(axis), axis=dim)
+    return lax.all_to_all(copies, axis, dim, dim, tiled=True)
 
 
 def copy_for_each(shard, axis):
@@ -192,7 +197,7 @@
     outgoing = jnp.take(padded_rows, table, axis=0).reshape(expert_count, capacity, width)
     arrived = lax.all_to_all(outgoing, "sp", split_axis=0, concat_axis=0, tiled=True)
     slots = arrived.shape[1]
-    fanned = lax.all_gather(arrived[None], "tp", axis=0, tiled=True)
+    fanned = tiled_gather(arrived[None], "tp", 0)
     shaped = fanned.reshape(tp_count, -1, local_count, slots, width)
     partial_value = expert_terms(
         shaped, "xslc", routed_gate_weight, routed_up_weight, routed_down_weight

time: 207 us -> 188 us (0.908)
  blocking collectives: 52.1 us -> 80.5 us
  waiting for transfers between devices: 58.8 us -> 31.1 us
  between operations: 14.3 us -> 0.87 us
  starting transfers between devices: 32 us -> 27.2 us
    all_to_all x0 -> x1, blocking collectives: none -> 28.6 us  [tiled_gather(): return lax.all_to_all(copies, axis, dim, dim, tiled=True)]
    all_gather x1 -> x0, waiting for transfers between devices: 27.8 us -> none  [shards(): fanned = lax.all_gather(arrived[None], 'tp', axis=0, tiled=True)]
    all_to_all x1, starting transfers between devices: 11.9 us -> 7.11 us  [shards(): lax.all_to_all(leaving, 'sp', split_axis=0, concat_axis=0, tiled=True)]
  transfers between devices with their start and end apart: 5 -> 4, of which waited for: 4 -> 3; matrix products, arithmetic and copies ran while one was open for 6% -> 6% of each run, Pallas kernels for 0% -> 0%
where the time goes in v1:
time: 188 us; the launch traced here: 187 us
  blocking collectives  80.5 us (43%)
  waiting for transfers between devices  31.1 us (17%)
  starting transfers between devices  27.2 us (14%)
  local copies, waits for them, and re-layouts  20.5 us (11%)
  matrix products  14 us (7%)
  other arithmetic  13.3 us (7%)
    all_to_all x1, blocking collectives, summed_on_arrival(): lax.all_to_all(cut_along(shard, dim, count), axis, 0, 0, tiled=True)  28.8 us
    all_to_all x1, blocking collectives, tiled_gather(): return lax.all_to_all(copies, axis, dim, dim, tiled=True)  28.6 us
    all_to_all x1, blocking collectives, shards(): lax.all_to_all(outgoing, 'sp', split_axis=0, concat_axis=0, tiled=True)  23.1 us
    all_to_all x1, waiting for transfers between devices, shards(): lax.all_to_all(leaving, 'sp', split_axis=0, concat_axis=0, tiled=True)  14.8 us
    all_to_all x1, starting transfers between devices, copy_for_each(): lax.all_to_all(jnp.broadcast_to(shard[None], (count, *shard.shape)), axis...  11.3 us
    all_to_all x1, waiting for transfers between devices, summed_on_arrival(): lax.all_to_all(cut_along(shard, dim, count), axis, 0, 0, tiled=True)  8.84 us
    all_to_all x1, waiting for transfers between devices, copy_for_each(): lax.all_to_all(jnp.broadcast_to(shard[None], (count, *shard.shape)), axis...  7.4 us
    all_to_all x1, starting transfers between devices, shards(): lax.all_to_all(leaving, 'sp', split_axis=0, concat_axis=0, tiled=True)  7.11 us
  transfers between devices with their start and end apart: 4, of which 3 were waited for; matrix products, arithmetic and copies ran while one was open for 6% of the time, Pallas kernels for 0%

profile of v1, /device:TPU:1, one launch (start us, length us, event | category | flops | bytes accessed | tf_op | source)
XLA Modules:
  0.0 187.5 jit_solution(10463653834387888441)
XLA Ops:
  0.0 1.1 copy.122
  1.1 4.5 %collective-permute-start = (bf16[3,2,256]{2,0,1:T(4,128)(2,1)S(1)}, bf16[3,2,256]{2,0,1:T(4,128)(2,1)S(1)}, u32[]{:S(2)}, u32[]{:S(2)}) collective-permute-start(bf16[3,2,256]{2,0,1:T(4,128)(2,1)S(1)} %slice.395), channel_id=1, source_target_pairs={{0,4},{4,8},{8,12},{12,16},{16,20},{20,24},{24,28},{28,32},{32,36}... | collective-permute-start | bytes 9224 | tf_op jit(solution)/shard_map/ppermute | solution.py:64
  5.6 0.7 convert_element_type.67
  6.3 0.7 fusion.66
  7.0 0.8 copy.139
  7.8 0.7 reshape.138
  8.5 0.1 fusion.27
  8.7 0.1 copy.124
  8.9 0.3 fusion.11
  9.2 0.1 copy.130
  9.3 0.1 copy.126
  9.4 0.3 fusion.7
  9.7 0.1 copy.155
  9.8 1.0 fusion.83
  10.8 0.2 fusion.35
  11.0 0.6 slice_bitcast_fusion
  11.6 0.6 fusion.81
  12.3 0.8 copy.156
  13.1 1.2 fusion.34
  14.4 0.7 broadcast_in_dim.59
  15.1 11.3 %all-to-all-start = ((f32[64,4,256]{2,1,0:T(4,128)}), f32[64,4,256]{2,1,0:T(4,128)S(1)}, u32[]{:S(2)}, u32[]{:S(2)}) async-start(f32[64,4,256]{2,1,0:T(4,128)} %broadcast_in_dim.59), calls=%async_computation | async-start | bytes 524288 | tf_op jit(solution)/shard_map/all_to_all | solution.py:17
  26.4 0.8 fusion.42
  27.3 0.3 reduce_window_sum.23
  27.5 0.9 select_reduce_fusion
  28.4 0.7 fusion.72
  29.1 1.4 scatter_custom_fusion
  30.6 0.7 slice.345
  31.3 0.7 slice.343
  32.1 7.4 %all-to-all-done = f32[64,4,256]{2,1,0:T(4,128)S(1)} async-done(((f32[64,4,256]{2,1,0:T(4,128)}), f32[64,4,256]{2,1,0:T(4,128)S(1)}, u32[]{:S(2)}, u32[]{:S(2)}) %all-to-all-start) | async-done | bytes 262176 | tf_op jit(solution)/shard_map/all_to_all | solution.py:17
  39.5 0.1 fusion.85
  39.7 0.6 slice.315
  40.4 0.7 slice.316
  41.1 0.9 fusion.91
  42.5 1.0 fusion.88
  45.2 1.3 fusion.1
  46.5 4.3 %all-to-all-start.1 = ((bf16[4,32,2048]{2,1,0:T(8,128)(2,1)}), bf16[4,32,2048]{2,1,0:T(8,128)(2,1)S(1)}, u32[]{:S(2)}, u32[]{:S(2)}) async-start(bf16[4,32,2048]{2,1,0:T(8,128)(2,1)} %bitcast.17), calls=%async_computation.1 | async-start | bytes 1048576 | tf_op jit(solution)/shard_map/all_to_all | solution.py:75
  50.8 0.1 broadcast_in_dim.63
  51.0 8.8 %all-to-all-done.1 = bf16[4,32,2048]{2,1,0:T(8,128)(2,1)S(1)} async-done(((bf16[4,32,2048]{2,1,0:T(8,128)(2,1)}), bf16[4,32,2048]{2,1,0:T(8,128)(2,1)S(1)}, u32[]{:S(2)}, u32[]{:S(2)}) %all-to-all-start.1) | async-done | bytes 524320 | tf_op jit(solution)/shard_map/all_to_all | solution.py:75
  60.0 0.2 fusion.53
  60.1 0.2 multiply_reduce_fusion.2
  60.3 0.1 add_convert_fusion.1
  60.5 0.9 gather_fusion
  61.4 1.1 gather.10
  62.6 1.6 broadcast_select_fusion
  64.2 23.1 %all_to_all.30 = bf16[64,2,2048]{2,1,0:T(2,128)(2,1)S(1)} all-to-all(bf16[64,2,2048]{2,1,0:T(2,128)(2,1)S(1)} %broadcast_select_fusion), channel_id=1, replica_groups=mesh['sp'=64,'tp'=4] {'sp'}, dimensions={0} | all-to-all | bytes 1048576 | tf_op jit(solution)/shard_map/all_to_all | solution.py:198
  87.3 0.2 copy.140
  87.4 0.2 concatenate.43
  87.7 28.6 %all_to_all.31 = bf16[4,64,2,2048]{3,1,2,0:T(8,128)(2,1)S(1)} all-to-all(bf16[4,64,2,2048]{3,1,2,0:T(8,128)(2,1)S(1)} %concatenate.43), channel_id=1, replica_groups=mesh['sp'=64,'tp'=4] {'tp'}, dimensions={0} | all-to-all | bytes 4194304 | tf_op jit(solution)/shard_map/all_to_all | solution.py:12
  116.4 1.3 copy-done.1
  117.7 0.7 convolution_bitcast_fusion.2
  118.4 5.5 %fusion = bf16[4,1,64,1,2,2048]{5,2,4,3,1,0:T(8,128)(2,1)} fusion(bf16[4,64,2,2048]{3,1,2,0:T(8,128)(2,1)} %copy-done.1, bf16[1,128,2048]{2,1,0:T(8,128)(2,1)} %param.36, bf16[1,2048,128]{2,1,0:T(8,128)(2,1)} %param.35, f32[4,64,1,2,128]{4,1,3,0,2:T(8,128)S(1)} %convolution_bitcast_fusion.2), kind=kOutput, calls=%fused_computation.4 | convolution fusion | flops 538312704 | bytes 5505024 | tf_op jit(solution)/shard_map/xslcf,lfd->xslcd/dot_general | solution.py:109
  123.9 28.8 %all_to_all.32 = bf16[4,1,64,1,2,2048]{5,2,4,3,1,0:T(8,128)(2,1)S(1)} all-to-all(bf16[4,1,64,1,2,2048]{5,2,4,3,1,0:T(8,128)(2,1)} %fusion), channel_id=1, replica_groups=mesh['sp'=64,'tp'=4] {'tp'}, dimensions={0} | all-to-all | bytes 4194304 | tf_op jit(solution)/shard_map/all_to_all | solution.py:75
  152.6 0.4 bitcast_reduce_fusion
  153.0 1.3 copy.143
  154.3 7.1 %all-to-all-start.5 = ((bf16[64,2,2048]{2,1,0:T(2,128)(2,1)}), bf16[64,2,2048]{2,1,0:T(2,128)(2,1)S(1)}, u32[]{:S(2)}, u32[]{:S(2)}) async-start(bf16[64,2,2048]{2,1,0:T(2,128)(2,1)} %copy.143), calls=%async_computation.5 | async-start | bytes 1048576 | tf_op jit(solution)/shard_map/all_to_all | solution.py:207
  161.6 2.7 %fusion.100 = f32[32,512]{1,0:T(8,128)} fusion(bf16[32,2048]{1,0:T(8,128)(2,1)S(1)} %add_convert_fusion.1, bf16[2048,512]{1,0:T(8,128)(2,1)} %param.37), kind=kOutput, calls=%fused_computation.188 | convolution fusion | flops 67108864 | bytes 2293760 | tf_op jit(solution)/shard_map/dot_general | solution.py:216
  164.3 14.8 %all-to-all-done.5 = bf16[64,2,2048]{2,1,0:T(2,128)(2,1)S(1)} async-done(((bf16[64,2,2048]{2,1,0:T(2,128)(2,1)}), bf16[64,2,2048]{2,1,0:T(2,128)(2,1)S(1)}, u32[]{:S(2)}, u32[]{:S(2)}) %all-to-all-start.5) | async-done | bytes 524320 | tf_op jit(solution)/shard_map/all_to_all | solution.py:207
  179.1 0.2 reshape.144
  179.3 1.7 gather_fusion.1
  181.1 1.4 reshape.145
  182.4 0.7 multiply_reduce_fusion
  183.2 3.3 %fusion.99 = (f32[32]{0:T(128)S(1)}, f32[32,2048]{1,0:T(8,128)S(1)}) fusion(f32[32,2048]{1,0:T(8,128)S(1)} %multiply_reduce_fusion, bf16[512,2048]{1,0:T(8,128)(2,1)} %param.39, bf16[32,2048]{1,0:T(8,128)(2,1)S(1)} %add_convert_fusion.1, bf16[2048,512]{1,0:T(8,128)(2,1)} %param.38, f32[32,512]{1,0:T(8,128)} %fusion.100), kind=kOutput, calls=%fused_computation.187 | convolution fusion | flops 134643680 | bytes 4915328 | tf_op jit(solution)/shard_map/dot_general | solution.py:219
  186.5 0.2 multiply_reduce_fusion.1
  186.7 0.8 add_convert_fusion
  (164 shorter events, 2.7 us)
Async XLA Ops:
  0.0 45.2 %copy-start = (bf16[2,256,2048]{2,1,0:T(8,128)(2,1)S(1)}, bf16[2,256,2048]{2,1,0:T(8,128)(2,1)}, u32[]{:S(2)}) copy-start(bf16[2,256,2048]{2,1,0:T(8,128)(2,1)} %param.29) | copy-start | bytes 6291460
  0.0 8.9 %copy-start.19 = (bf16[2,4,64,64]{3,2,1,0:T(8,128)(2,1)S(1)}, bf16[2,4,64,64]{3,2,1,0:T(8,128)(2,1)}, u32[]{:S(2)}) copy-start(bf16[2,4,64,64]{3,2,1,0:T(8,128)(2,1)} %param.25) | copy-start | bytes 196612
  1.1 7.4 %collective-permute-start = (bf16[3,2,256]{2,0,1:T(4,128)(2,1)S(1)}, bf16[3,2,256]{2,0,1:T(4,128)(2,1)S(1)}, u32[]{:S(2)}, u32[]{:S(2)}) collective-permute-start(bf16[3,2,256]{2,0,1:T(4,128)(2,1)S(1)} %slice.395), channel_id=1, source_target_pairs={{0,4},{4,8},{8,12},{12,16},{16,20},{20,24},{24,28},{28,32},{32,36}... | collective-permute-start | bytes 9224 | tf_op jit(solution)/shard_map/ppermute | solution.py:64
  6.3 2.5 %copy-start.7 = (f32[2,256]{1,0:T(2,128)}, f32[2,256]{1,0:T(2,128)S(1)}, u32[]{:S(2)}) copy-start(f32[2,256]{1,0:T(2,128)S(1)} %get-tuple-element.37) | copy-start | bytes 6148
  6.3 2.5 %copy-start.8 = (f32[2,256]{1,0:T(2,128)}, f32[2,256]{1,0:T(2,128)S(1)}, u32[]{:S(2)}) copy-start(f32[2,256]{1,0:T(2,128)S(1)} %get-tuple-element.38) | copy-start | bytes 6148
  6.3 2.5 %copy-start.9 = (f32[2,256]{1,0:T(2,128)}, f32[2,256]{1,0:T(2,128)S(1)}, u32[]{:S(2)}) copy-start(f32[2,256]{1,0:T(2,128)S(1)} %get-tuple-element.39) | copy-start | bytes 6148
  6.3 2.5 %copy-start.10 = (f32[2,256]{1,0:T(2,128)}, f32[2,256]{1,0:T(2,128)S(1)}, u32[]{:S(2)}) copy-start(f32[2,256]{1,0:T(2,128)S(1)} %get-tuple-element.40) | copy-start | bytes 6148
  8.5 0.9 copy-start.20
  13.1 1.2 copy-start.15
  15.1 24.4 %all-to-all-start = ((f32[64,4,256]{2,1,0:T(4,128)}), f32[64,4,256]{2,1,0:T(4,128)S(1)}, u32[]{:S(2)}, u32[]{:S(2)}) async-start(f32[64,4,256]{2,1,0:T(4,128)} %broadcast_in_dim.59), calls=%async_computation | async-start | bytes 524288 | tf_op jit(solution)/shard_map/all_to_all | solution.py:17
  29.1 13.0 %copy-start.17 = (s32[128]{0:T(128)}, s32[128]{0:T(128)S(1)}, u32[]{:S(2)}) copy-start(s32[128]{0:T(128)S(1)} %fusion.72) | copy-start | bytes 1540
  42.4 1.2 copy-start.5
  43.8 1.2 copy-start.6
  44.3 0.9 copy-start.4
  45.2 5.6 %copy-start.21 = (s32[128]{0:T(128)S(1)}, s32[128]{0:T(128)}, u32[]{:S(2)}) copy-start(s32[128]{0:T(128)} %scatter_custom_fusion) | copy-start | bytes 1540
  45.2 14.7 %copy-start.2 = (bf16[32,2048]{1,0:T(8,128)(2,1)S(1)}, bf16[32,2048]{1,0:T(8,128)(2,1)}, u32[]{:S(2)}) copy-start(bf16[32,2048]{1,0:T(8,128)(2,1)} %param.21) | copy-start | bytes 393220
  46.5 13.8 %copy-start.11 = (f32[2048]{0:T(1024)S(1)}, f32[2048]{0:T(1024)}, u32[]{:S(2)}) copy-start(f32[2048]{0:T(1024)} %param.31) | copy-start | bytes 24580
  46.5 13.8 %copy-start.12 = (f32[2048]{0:T(1024)S(1)}, f32[2048]{0:T(1024)}, u32[]{:S(2)}) copy-start(f32[2048]{0:T(1024)} %param.30) | copy-start | bytes 24580
  46.5 13.3 %all-to-all-start.1 = ((bf16[4,32,2048]{2,1,0:T(8,128)(2,1)}), bf16[4,32,2048]{2,1,0:T(8,128)(2,1)S(1)}, u32[]{:S(2)}, u32[]{:S(2)}) async-start(bf16[4,32,2048]{2,1,0:T(8,128)(2,1)} %bitcast.17), calls=%async_computation.1 | async-start | bytes 1048576 | tf_op jit(solution)/shard_map/all_to_all | solution.py:75
  87.7 30.0 %copy-start.3 = (bf16[1,2048,128]{2,1,0:T(8,128)(2,1)S(1)}, bf16[1,2048,128]{2,1,0:T(8,128)(2,1)}, u32[]{:S(2)}) copy-start(bf16[1,2048,128]{2,1,0:T(8,128)(2,1)} %param.34) | copy-start | bytes 1572868
  116.3 1.3 copy-start.1
  152.6 8.8 %copy-start.16 = (f32[128,4]{0,1:T(4,128)S(1)}, f32[128,4]{0,1:T(4,128)}, u32[]{:S(2)}) copy-start(f32[128,4]{0,1:T(4,128)} %param.33) | copy-start | bytes 6148
  152.6 9.0 %copy-start.18 = (s32[128]{0:T(128)S(1)}, s32[128]{0:T(128)}, u32[]{:S(2)}) copy-start(s32[128]{0:T(128)} %copy-done.17) | copy-start | bytes 1540
  154.3 24.8 %all-to-all-start.5 = ((bf16[64,2,2048]{2,1,0:T(2,128)(2,1)}), bf16[64,2,2048]{2,1,0:T(2,128)(2,1)S(1)}, u32[]{:S(2)}, u32[]{:S(2)}) async-start(bf16[64,2,2048]{2,1,0:T(2,128)(2,1)} %copy.143), calls=%async_computation.5 | async-start | bytes 1048576 | tf_op jit(solution)/shard_map/all_to_all | solution.py:207
  183.2 3.5 %copy-start.13 = (f32[2048]{0:T(1024)S(1)}, f32[2048]{0:T(1024)}, u32[]{:S(2)}) copy-start(f32[2048]{0:T(1024)} %param.41) | copy-start | bytes 24580
  183.2 3.5 %copy-start.14 = (f32[2048]{0:T(1024)S(1)}, f32[2048]{0:T(1024)}, u32[]{:S(2)}) copy-start(f32[2048]{0:T(1024)} %param.40) | copy-start | bytes 24580
